TPU v7x, 256 devices: a whole 4x4x8 slice. The times are simulated.
256 devices in a mesh: ep: 16 (over y, x), tp: 16 (over z, core).
Axes of the slice: x: 4, y: 4, z: 8, core: 2. Of those that a mesh axis runs over, the one named last changes fastest.
Arguments:
- tokens: bfloat16 [512, 2048], P('ep', 'tp'), may hold values from -80 to 80
- delta_state: float32 [512, 16, 128, 128], P('ep', 'tp'), may hold values from -1.8 to 1.8
- mix_gain: bfloat16 [2048], replicated, may hold values from 0.099609375 to 1.8984375
- w_query: bfloat16 [2048, 2048], P(None, 'tp'), may hold values from -0.125 to 0.125
- w_key: bfloat16 [2048, 2048], P(None, 'tp'), may hold values from -0.125 to 0.125
- w_value: bfloat16 [2048, 2048], P(None, 'tp'), may hold values from -0.125 to 0.125
- w_outgate: bfloat16 [2048, 2048], P(None, 'tp'), may hold values from -0.125 to 0.125
- w_beta: bfloat16 [2048, 16], P(None, 'tp'), may hold values from -0.125 to 0.125
- w_decay: bfloat16 [2048, 16], P(None, 'tp'), may hold values from -0.125 to 0.125
- decay_scale: float32 [16], P('tp'), may hold values from 0.05 to 1.5
- decay_bias: float32 [16], P('tp'), may hold values from -1.5 to 1.5
- head_gain: bfloat16 [128], replicated, may hold values from 0.099609375 to 1.8984375
- w_output: bfloat16 [2048, 2048], P('tp'), may hold values from -0.125 to 0.125
- ffn_gain: bfloat16 [2048], replicated, may hold values from 0.099609375 to 1.8984375
- route_ids: int32 [512, 6], P('ep'), may hold values from 0 to 255, all different within a row; in each aligned block of 32 rows (0 to 31, 32 to 63, ...) at most 2 rows name the same one
- route_weights: float32 [512, 6], P('ep'), may hold values from 0.2 to 1.2
- expert_gate: bfloat16 [256, 2048, 512], P(('ep', 'tp')), may hold values from -0.125 to 0.125
- expert_up: bfloat16 [256, 2048, 512], P(('ep', 'tp')), may hold values from -0.125 to 0.125
- expert_down: bfloat16 [256, 512, 2048], P(('ep', 'tp')), may hold values from -0.25 to 0.25
- shared_gate: bfloat16 [2048, 512], P(None, 'tp'), may hold values from -0.125 to 0.125
- shared_up: bfloat16 [2048, 512], P(None, 'tp'), may hold values from -0.125 to 0.125
- shared_down: bfloat16 [512, 2048], P('tp'), may hold values from -0.25 to 0.25
Outputs:
- layer_out: bfloat16 [512, 2048], P('ep', 'tp')
- new_state: float32 [512, 16, 128, 128], P('ep', 'tp')
Inputs may be any that keep to these rules, and one draw needn't show every extreme that they name: `route_ids`: each row names 6 different experts. In each aligned block of 32 rows (the sequences of one index of ep) no expert is named by more than 2 rows, and in every draw some expert is named by exactly 2 rows of some block.
All inputs are finite; a program needn't handle non-finite values.
Results may differ from a plain program's by a relative error of at most 0.013.
Values may be sent and summed in bfloat16 or wider, within the bound.
A program may use at most 64 MiB of HBM per device.

v0:
```python
import jax
import jax.numpy as jnp
from jax import lax
from jax.sharding import PartitionSpec as P

epsilon = 1e-06


def copy_for_each(array, axis):
    length = lax.axis_size(axis)
    return lax.all_to_all(
        jnp.broadcast_to(array[None], (length, *array.shape)), axis, 0, 0, tiled=True
    )


def in_order(parts, dim):
    parts = jnp.moveaxis(parts, 0, dim)
    lengths = parts.shape
    return parts.reshape(*lengths[:dim], lengths[dim] * lengths[dim + 1], *lengths[dim + 2 :])


def collect(array, axis, dim):
    parts = copy_for_each(array, axis)
    return in_order(parts, dim)


def in_blocks(array, dim, length):
    before, after = (array.shape[:dim], array.shape[dim + 1 :])
    return jnp.moveaxis(array.reshape(*before, length, -1, *after), dim, 0)


def summed_on_arrival(array, axis, dim):
    parts = in_blocks(array, dim, lax.axis_size(axis))
    arrived = lax.all_to_all(parts, axis, split_axis=0, concat_axis=0, tiled=True)
    return arrived.astype(jnp.float32).sum(axis=0)


def of_everyone(array, axis):
    everything = copy_for_each(array, axis)
    return jnp.sum(everything, axis=0)


def rms_norm(values, gain_vector):
    squares = jnp.mean(values * values, axis=-1, keepdims=True)
    return values * lax.rsqrt(squares + epsilon) * gain_vector.astype(jnp.float32)


def unit_rows(values):
    return values * lax.rsqrt(jnp.sum(values * values, axis=-1, keepdims=True) + epsilon)


def expert_block(rows, expert_gate, expert_up, expert_down):
    gate_part = jnp.einsum("sjnd,jdf->sjnf", rows, expert_gate, preferred_element_type=jnp.float32)
    up_part = jnp.einsum("sjnd,jdf->sjnf", rows, expert_up, preferred_element_type=jnp.float32)
    hidden = (jax.nn.silu(gate_part) * up_part).astype(jnp.bfloat16)
    outputs = jnp.einsum("sjnf,jfd->sjnd", hidden, expert_down, preferred_element_type=jnp.float32)
    return outputs.astype(jnp.bfloat16)


def body(
    tokens,
    delta_state,
    mix_gain,
    w_query,
    w_key,
    w_value,
    w_outgate,
    w_beta,
    w_decay,
    decay_scale,
    decay_bias,
    head_gain,
    w_output,
    ffn_gain,
    route_ids,
    route_weights,
    expert_gate,
    expert_up,
    expert_down,
    shared_gate,
    shared_up,
    shared_down,
):
    rows_count = tokens.shape[0]
    width_own = tokens.shape[1]
    heads_here = delta_state.shape[1]
    key_size = delta_state.shape[2]
    tp_index = lax.axis_index("tp")
    full_rows = collect(tokens, "tp", 1)
    resid_in = full_rows.astype(jnp.float32)
    normed_mix = rms_norm(resid_in, mix_gain).astype(jnp.bfloat16)

    def project(weight):
        result = jnp.dot(normed_mix, weight, preferred_element_type=jnp.float32)
        result = lax.optimization_barrier(result.astype(jnp.bfloat16)).astype(jnp.float32)
        return result.reshape(rows_count, heads_here, -1)

    query_unit = unit_rows(project(w_query)) * key_size ** (-0.5)
    key_unit = unit_rows(project(w_key))
    values_new = project(w_value)
    out_gate = project(w_outgate)
    beta_gate = jax.nn.sigmoid(jnp.dot(normed_mix, w_beta, preferred_element_type=jnp.float32))
    decay_input = jnp.dot(normed_mix, w_decay, preferred_element_type=jnp.float32) + decay_bias
    decay_rate = jnp.exp(-decay_scale * jax.nn.softplus(decay_input))
    key_read = jnp.einsum("shk,shkv->shv", key_unit, delta_state)
    written = beta_gate[:, :, None] * key_unit
    kept_state = delta_state - written[:, :, :, None] * key_read[:, :, None, :]
    new_state = (
        decay_rate[:, :, None, None] * kept_state
        + written[:, :, :, None] * values_new[:, :, None, :]
    )
    state_read = jnp.einsum("shk,shkv->shv", query_unit, new_state)
    gated = (
        (rms_norm(state_read, head_gain) * jax.nn.silu(out_gate))
        .reshape(rows_count, -1)
        .astype(jnp.bfloat16)
    )
    partial_value = jnp.dot(gated, w_output, preferred_element_type=jnp.float32)
    mixed_own = summed_on_arrival(partial_value.astype(jnp.bfloat16), "tp", 1)
    resid_own = tokens.astype(jnp.float32) + mixed_own
    gain_own = lax.dynamic_slice_in_dim(ffn_gain, tp_index * width_own, width_own, 0)
    square_sum = of_everyone(jnp.sum(resid_own * resid_own, axis=1), "tp")
    row_scale = lax.rsqrt(square_sum / (width_own * lax.axis_size("tp")) + epsilon)
    normed_own = (resid_own * row_scale[:, None] * gain_own.astype(jnp.float32)).astype(
        jnp.bfloat16
    )
    normed_ffn = collect(normed_own, "tp", 1)
    model_width = normed_ffn.shape[1]
    ep_count = lax.axis_size("ep")
    tp_count = lax.axis_size("tp")
    experts_here = expert_gate.shape[0]
    top_count = route_ids.shape[1]
    expert_total = experts_here * ep_count * tp_count
    capacity = max(2, 8 * rows_count * top_count // (3 * expert_total))
    pair_count = rows_count * top_count
    flat_ids = route_ids.reshape(pair_count)
    owner_ep = flat_ids // (tp_count * experts_here)
    owner_tp = flat_ids // experts_here % tp_count
    local_slot = flat_ids % experts_here
    mine_mask = owner_tp == tp_index
    pair_weights = jnp.where(mine_mask, route_weights.reshape(pair_count), 0.0)
    pair_index = jnp.arange(pair_count, dtype=jnp.int32)
    earlier = (flat_ids[:, None] == flat_ids[None, :]) & (pair_index[None, :] < pair_index[:, None])
    slot_rank = jnp.sum(earlier.astype(jnp.int32), axis=1)
    slot_count = ep_count * experts_here * capacity
    target = jnp.where(mine_mask, (owner_ep * experts_here + local_slot) * capacity + slot_rank, -1)
    choose = (target[:, None] == jnp.arange(slot_count, dtype=jnp.int32)[None, :]).astype(
        jnp.bfloat16
    )
    by_row = jnp.sum(choose.reshape(rows_count, top_count, slot_count), axis=1)
    outgoing = jnp.einsum("sb,sd->bd", by_row, normed_ffn, preferred_element_type=jnp.float32)
    outgoing = outgoing.astype(jnp.bfloat16).reshape(ep_count, experts_here, capacity, model_width)
    results = expert_block(
        lax.all_to_all(outgoing, "ep", split_axis=0, concat_axis=0, tiled=True),
        expert_gate,
        expert_up,
        expert_down,
    )
    returned = lax.all_to_all(results, "ep", split_axis=0, concat_axis=0, tiled=True)
    picked = jnp.dot(
        choose, returned.reshape(slot_count, model_width), preferred_element_type=jnp.float32
    )
    routed = jnp.sum(
        (pair_weights[:, None] * picked).reshape(rows_count, top_count, model_width), axis=1
    )
    shared_gate_part = jnp.dot(normed_ffn, shared_gate, preferred_element_type=jnp.float32)
    shared_up_part = jnp.dot(normed_ffn, shared_up, preferred_element_type=jnp.float32)
    hidden_shared = (jax.nn.silu(shared_gate_part) * shared_up_part).astype(jnp.bfloat16)
    branch_sum = routed + jnp.dot(hidden_shared, shared_down, preferred_element_type=jnp.float32)
    combined = summed_on_arrival(branch_sum.astype(jnp.bfloat16), "tp", 1)
    layer_out = (resid_own + combined).astype(jnp.bfloat16)
    return (layer_out, new_state)


def solution(mesh):
    return jax.shard_map(
        body,
        mesh=mesh,
        in_specs=(
            P("ep", "tp"),
            P("ep", "tp", None, None),
            P(),
            P(None, "tp"),
            P(None, "tp"),
            P(None, "tp"),
            P(None, "tp"),
            P(None, "tp"),
            P(None, "tp"),
            P("tp"),
            P("tp"),
            P(),
            P("tp", None),
            P(),
            P("ep", None),
            P("ep", None),
            P(("ep", "tp"), None, None),
            P(("ep", "tp"), None, None),
            P(("ep", "tp"), None, None),
            P(None, "tp"),
            P(None, "tp"),
            P("tp", None),
        ),
        out_specs=(P("ep", "tp"), P("ep", "tp", None, None)),
        check_vma=False,
    )
```

profile of v0, /device:TPU:1, one launch (start us, length us, event | category | flops | bytes accessed | tf_op | source)
XLA Modules:
  0.0 119.4 jit_solution(16285853830914806829)
XLA Ops:
  0.7 1.5 %broadcast_in_dim.10 = bf16[16,32,128]{2,1,0:T(8,128)(2,1)} broadcast(bf16[32,128]{1,0:T(8,128)(2,1)} %param.22), dimensions={1,2} | broadcast | bytes 139264 | tf_op jit(solution)/shard_map/broadcast_in_dim | solution.py:12
  2.2 10.0 %all-to-all-start = ((bf16[16,32,128]{2,1,0:T(8,128)(2,1)}), bf16[16,32,128]{2,1,0:T(8,128)(2,1)S(1)}, u32[]{:S(2)}, u32[]{:S(2)}) async-start(bf16[16,32,128]{2,1,0:T(8,128)(2,1)} %broadcast_in_dim.10), calls=%async_computation | async-start | bytes 262144 | tf_op jit(solution)/shard_map/all_to_all | solution.py:11
  15.7 5.4 %all-to-all-done = bf16[16,32,128]{2,1,0:T(8,128)(2,1)S(1)} async-done(((bf16[16,32,128]{2,1,0:T(8,128)(2,1)}), bf16[16,32,128]{2,1,0:T(8,128)(2,1)S(1)}, u32[]{:S(2)}, u32[]{:S(2)}) %all-to-all-start) | async-done | bytes 131104 | tf_op jit(solution)/shard_map/all_to_all | solution.py:11
  21.2 1.4 %convolution_convert_fusion.5 = bf16[32,128]{1,0:T(8,128)(2,1)S(1)} fusion(bf16[2048,128]{1,0:T(8,128)(2,1)} %param.26, f32[2048]{0:T(1024)S(1)} %get-tuple-element.7, f32[32]{0:T(128)S(1)} %add_rsqrt_fusion.4, bf16[16,32,128]{2,1,0:T(8,128)(2,1)S(1)} %all-to-all-done), kind=kOutput, calls=%fused_computation.28 | convolution fusion | flops 17043456 | bytes 671872 | tf_op jit(solution)/shard_map/dot_general | solution.py:94
  22.7 1.3 %convolution_convert_fusion.6 = bf16[32,128]{1,0:T(8,128)(2,1)S(1)} fusion(bf16[2048,128]{1,0:T(8,128)(2,1)} %param.25, f32[2048]{0:T(1024)S(1)} %get-tuple-element.7, f32[32]{0:T(128)S(1)} %add_rsqrt_fusion.4, bf16[16,32,128]{2,1,0:T(8,128)(2,1)S(1)} %all-to-all-done), kind=kOutput, calls=%fused_computation.29 | convolution fusion | flops 17043456 | bytes 671872 | tf_op jit(solution)/shard_map/dot_general | solution.py:94
  24.3 1.3 %convolution_convert_fusion.4 = bf16[32,128]{1,0:T(8,128)(2,1)S(1)} fusion(bf16[2048,128]{1,0:T(8,128)(2,1)} %param.27, f32[2048]{0:T(1024)S(1)} %get-tuple-element.7, f32[32]{0:T(128)S(1)} %add_rsqrt_fusion.4, bf16[16,32,128]{2,1,0:T(8,128)(2,1)S(1)} %all-to-all-done), kind=kOutput, calls=%fused_computation.27 | convolution fusion | flops 17043456 | bytes 671872 | tf_op jit(solution)/shard_map/dot_general | solution.py:94
  28.9 3.4 %all-to-all-start.1 = ((bf16[16,32,128]{2,1,0:T(8,128)(2,1)}), bf16[16,32,128]{2,1,0:T(8,128)(2,1)S(1)}, u32[]{:S(2)}, u32[]{:S(2)}) async-start(bf16[16,32,128]{2,1,0:T(8,128)(2,1)} %bitcast.221), calls=%async_computation.1 | async-start | bytes 262144 | tf_op jit(solution)/shard_map/all_to_all | solution.py:34
  32.6 8.6 %all-to-all-done.1 = bf16[16,32,128]{2,1,0:T(8,128)(2,1)S(1)} async-done(((bf16[16,32,128]{2,1,0:T(8,128)(2,1)}), bf16[16,32,128]{2,1,0:T(8,128)(2,1)S(1)}, u32[]{:S(2)}, u32[]{:S(2)}) %all-to-all-start.1) | async-done | bytes 131104 | tf_op jit(solution)/shard_map/all_to_all | solution.py:34
  42.0 3.4 %all-to-all-start.2 = ((f32[16,1,32]{2,1,0:T(1,128)}), f32[16,1,32]{2,1,0:T(1,128)S(1)}, u32[]{:S(2)}, u32[]{:S(2)}) async-start(f32[16,1,32]{2,1,0:T(1,128)} %broadcast_in_dim.12), calls=%async_computation.2 | async-start | bytes 16384 | tf_op jit(solution)/shard_map/all_to_all | solution.py:11
  46.2 5.7 %all-to-all-done.2 = f32[16,1,32]{2,1,0:T(1,128)S(1)} async-done(((f32[16,1,32]{2,1,0:T(1,128)}), f32[16,1,32]{2,1,0:T(1,128)S(1)}, u32[]{:S(2)}, u32[]{:S(2)}) %all-to-all-start.2) | async-done | bytes 2080 | tf_op jit(solution)/shard_map/all_to_all | solution.py:11
  52.7 4.0 %all-to-all-start.3 = ((bf16[16,32,128]{2,1,0:T(8,128)(2,1)}), bf16[16,32,128]{2,1,0:T(8,128)(2,1)S(1)}, u32[]{:S(2)}, u32[]{:S(2)}) async-start(bf16[16,32,128]{2,1,0:T(8,128)(2,1)} %broadcast_in_dim.13), calls=%async_computation.3 | async-start | bytes 262144 | tf_op jit(solution)/shard_map/all_to_all | solution.py:11
  57.0 8.9 %all-to-all-done.3 = bf16[16,32,128]{2,1,0:T(8,128)(2,1)S(1)} async-done(((bf16[16,32,128]{2,1,0:T(8,128)(2,1)}), bf16[16,32,128]{2,1,0:T(8,128)(2,1)S(1)}, u32[]{:S(2)}, u32[]{:S(2)}) %all-to-all-start.3) | async-done | bytes 131104 | tf_op jit(solution)/shard_map/all_to_all | solution.py:11
  66.8 6.8 %all-to-all-start.4 = ((bf16[16,1,2,2048]{3,2,1,0:T(2,128)(2,1)}), bf16[16,1,2,2048]{3,2,1,0:T(2,128)(2,1)S(1)}, u32[]{:S(2)}, u32[]{:S(2)}) async-start(bf16[16,1,2,2048]{3,2,1,0:T(2,128)(2,1)} %bitcast.20), calls=%async_computation.4 | async-start | bytes 262144 | tf_op jit(solution)/shard_map/all_to_all | solution.py:154
  73.6 7.3 %all-to-all-done.4 = bf16[16,1,2,2048]{3,2,1,0:T(2,128)(2,1)S(1)} async-done(((bf16[16,1,2,2048]{3,2,1,0:T(2,128)(2,1)}), bf16[16,1,2,2048]{3,2,1,0:T(2,128)(2,1)S(1)}, u32[]{:S(2)}, u32[]{:S(2)}) %all-to-all-start.4) | async-done | bytes 131104 | tf_op jit(solution)/shard_map/all_to_all | solution.py:154
  80.9 2.0 %fusion.13 = f32[16,1,2,512]{3,0,2,1:T(8,128)S(1)} fusion(bf16[1,2048,512]{2,1,0:T(8,128)(2,1)} %param.38, bf16[16,1,2,2048]{3,2,1,0:T(2,128)(2,1)S(1)} %all-to-all-done.4), kind=kOutput, calls=%fused_computation.19 | convolution fusion | flops 67108864 | bytes 2293760 | tf_op jit(solution)/shard_map/sjnd,jdf->sjnf/dot_general | solution.py:53
  83.0 2.5 %fusion.1 = bf16[16,1,2,2048]{3,0,2,1:T(8,128)(2,1)S(1)} fusion(bf16[1,512,2048]{2,1,0:T(8,128)(2,1)S(1)} %copy-done, bf16[1,2048,512]{2,1,0:T(8,128)(2,1)} %param.39, bf16[16,1,2,2048]{3,2,1,0:T(2,128)(2,1)S(1)} %all-to-all-done.4, f32[16,1,2,512]{3,0,2,1:T(8,128)S(1)} %fusion.13), kind=kOutput, calls=%fused_computation.6 | convolution fusion | flops 134381568 | bytes 4521984 | tf_op jit(solution)/shard_map/sjnf,jfd->sjnd/dot_general | solution.py:56
  86.3 3.5 %all-to-all-start.5 = ((bf16[16,1,2,2048]{3,2,1,0:T(2,128)(2,1)}), bf16[16,1,2,2048]{3,2,1,0:T(2,128)(2,1)S(1)}, u32[]{:S(2)}, u32[]{:S(2)}) async-start(bf16[16,1,2,2048]{3,2,1,0:T(2,128)(2,1)} %copy.77), calls=%async_computation.5 | async-start | bytes 262144 | tf_op jit(solution)/shard_map/all_to_all | solution.py:159
  90.0 6.6 %all-to-all-done.5 = bf16[16,1,2,2048]{3,2,1,0:T(2,128)(2,1)S(1)} async-done(((bf16[16,1,2,2048]{3,2,1,0:T(2,128)(2,1)}), bf16[16,1,2,2048]{3,2,1,0:T(2,128)(2,1)S(1)}, u32[]{:S(2)}, u32[]{:S(2)}) %all-to-all-start.5) | async-done | bytes 131104 | tf_op jit(solution)/shard_map/all_to_all | solution.py:159
  96.7 1.6 %convolution_multiply_fusion = f32[192,2048]{1,0:T(8,128)} fusion(bf16[32,2048]{1,0:T(8,128)(2,1)S(1)} %reshape.314, f32[192]{0:T(256)S(1)} %broadcast_select_fusion, s32[192]{0:T(256)S(1)} %get-tuple-element.2), kind=kOutput, calls=%fused_computation | convolution fusion | flops 25565184 | bytes 1705472 | tf_op jit(solution)/shard_map/dot_general | solution.py:160
  98.3 2.6 %reshape.315 = f32[32,6,2048]{2,1,0:T(8,128)} reshape(f32[192,2048]{1,0:T(8,128)} %convolution_multiply_fusion) | data formatting | bytes 3145728 | tf_op jit(solution)/shard_map/reshape | solution.py:164
  100.9 2.3 %reduce_sum.114 = f32[32,2048]{1,0:T(8,128)S(1)} reduce(f32[32,6,2048]{2,1,0:T(8,128)} %reshape.315, f32[]{:T(128)} %constant.69.clone.1), dimensions={1}, to_apply=%region_9.10 | reduce | flops 327680 | bytes 1835012 | tf_op jit(solution)/shard_map/reduce_sum | solution.py:163
  104.3 5.4 %all-to-all-start.6 = ((bf16[16,32,128]{2,1,0:T(8,128)(2,1)}), bf16[16,32,128]{2,1,0:T(8,128)(2,1)S(1)}, u32[]{:S(2)}, u32[]{:S(2)}) async-start(bf16[16,32,128]{2,1,0:T(8,128)(2,1)} %bitcast.219), calls=%async_computation.6 | async-start | bytes 262144 | tf_op jit(solution)/shard_map/all_to_all | solution.py:34
  109.6 2.9 %multiply_add_fusion = f32[32,1,128,128]{3,2,1,0:T(8,128)} fusion(f32[32,1,128,128]{3,2,1,0:T(8,128)} %param.23, f32[32,128]{1,0:T(8,128)S(1)} %convert_element_type.122, f32[32,128]{1,0:T(8,128)S(1)} %bitcast.224, f32[32,128]{1,0:T(8,128)S(1)} %get-tuple-element.4, f32[32]{0:T(128)S(1)} %fusion.99), kind=kLoop, calls=%fused_computation.16 | loop fusion | flops 2621440 | bytes 4243584 | tf_op jit(solution)/shard_map/add | solution.py:109
  112.6 6.2 %all-to-all-done.6 = bf16[16,32,128]{2,1,0:T(8,128)(2,1)S(1)} async-done(((bf16[16,32,128]{2,1,0:T(8,128)(2,1)}), bf16[16,32,128]{2,1,0:T(8,128)(2,1)S(1)}, u32[]{:S(2)}, u32[]{:S(2)}) %all-to-all-start.6) | async-done | bytes 131104 | tf_op jit(solution)/shard_map/all_to_all | solution.py:34
  (70 shorter events, 12.6 us)
Async XLA Ops:
  0.6 82.4 %copy-start = (bf16[1,512,2048]{2,1,0:T(8,128)(2,1)S(1)}, bf16[1,512,2048]{2,1,0:T(8,128)(2,1)}, u32[]{:S(2)}) copy-start(bf16[1,512,2048]{2,1,0:T(8,128)(2,1)} %param.40) | copy-start | bytes 6291460
  0.6 24.9 %copy-start.9 = (bf16[2048,1]{0,1:T(2,128)(2,1)S(1)}, bf16[2048,1]{0,1:T(2,128)(2,1)}, u32[]{:S(2)}) copy-start(bf16[2048,1]{0,1:T(2,128)(2,1)} %param.29) | copy-start | bytes 12292
  2.2 18.9 %all-to-all-start = ((bf16[16,32,128]{2,1,0:T(8,128)(2,1)}), bf16[16,32,128]{2,1,0:T(8,128)(2,1)S(1)}, u32[]{:S(2)}, u32[]{:S(2)}) async-start(bf16[16,32,128]{2,1,0:T(8,128)(2,1)} %broadcast_in_dim.10), calls=%async_computation | async-start | bytes 262144 | tf_op jit(solution)/shard_map/all_to_all | solution.py:11
  21.0 4.9 %copy-start.1 = (f32[32,1,128,128]{3,2,1,0:T(8,128)S(1)}, f32[32,1,128,128]{3,2,1,0:T(8,128)}, u32[]{:S(2)}) copy-start(f32[32,1,128,128]{3,2,1,0:T(8,128)} %param.23) | copy-start | bytes 6291460
  22.6 3.7 %copy-start.10 = (bf16[2048,1]{0,1:T(2,128)(2,1)S(1)}, bf16[2048,1]{0,1:T(2,128)(2,1)}, u32[]{:S(2)}) copy-start(bf16[2048,1]{0,1:T(2,128)(2,1)} %param.30) | copy-start | bytes 12292
  26.3 1.4 %copy-start.2 = (bf16[2048,128]{1,0:T(8,128)(2,1)S(1)}, bf16[2048,128]{1,0:T(8,128)(2,1)}, u32[]{:S(2)}) copy-start(bf16[2048,128]{1,0:T(8,128)(2,1)} %param.28) | copy-start | bytes 1572868
  26.3 1.6 %copy-start.3 = (bf16[128,2048]{1,0:T(8,128)(2,1)S(1)}, bf16[128,2048]{1,0:T(8,128)(2,1)}, u32[]{:S(2)}) copy-start(bf16[128,2048]{1,0:T(8,128)(2,1)} %param.34) | copy-start | bytes 1572868
  26.6 14.7 %copy-start.7 = (bf16[32,128]{1,0:T(8,128)(2,1)S(1)}, bf16[32,128]{1,0:T(8,128)(2,1)}, u32[]{:S(2)}) copy-start(bf16[32,128]{1,0:T(8,128)(2,1)} %param.22) | copy-start | bytes 24580
  26.6 30.2 %copy-start.8 = (f32[32,6]{0,1:T(8,128)S(1)}, f32[32,6]{0,1:T(8,128)}, u32[]{:S(2)}) copy-start(f32[32,6]{0,1:T(8,128)} %param.37) | copy-start | bytes 2308
  28.9 12.3 %all-to-all-start.1 = ((bf16[16,32,128]{2,1,0:T(8,128)(2,1)}), bf16[16,32,128]{2,1,0:T(8,128)(2,1)S(1)}, u32[]{:S(2)}, u32[]{:S(2)}) async-start(bf16[16,32,128]{2,1,0:T(8,128)(2,1)} %bitcast.221), calls=%async_computation.1 | async-start | bytes 262144 | tf_op jit(solution)/shard_map/all_to_all | solution.py:34
  42.0 9.9 %all-to-all-start.2 = ((f32[16,1,32]{2,1,0:T(1,128)}), f32[16,1,32]{2,1,0:T(1,128)S(1)}, u32[]{:S(2)}, u32[]{:S(2)}) async-start(f32[16,1,32]{2,1,0:T(1,128)} %broadcast_in_dim.12), calls=%async_computation.2 | async-start | bytes 16384 | tf_op jit(solution)/shard_map/all_to_all | solution.py:11
  52.7 13.2 %all-to-all-start.3 = ((bf16[16,32,128]{2,1,0:T(8,128)(2,1)}), bf16[16,32,128]{2,1,0:T(8,128)(2,1)S(1)}, u32[]{:S(2)}, u32[]{:S(2)}) async-start(bf16[16,32,128]{2,1,0:T(8,128)(2,1)} %broadcast_in_dim.13), calls=%async_computation.3 | async-start | bytes 262144 | tf_op jit(solution)/shard_map/all_to_all | solution.py:11
  66.8 14.1 %all-to-all-start.4 = ((bf16[16,1,2,2048]{3,2,1,0:T(2,128)(2,1)}), bf16[16,1,2,2048]{3,2,1,0:T(2,128)(2,1)S(1)}, u32[]{:S(2)}, u32[]{:S(2)}) async-start(bf16[16,1,2,2048]{3,2,1,0:T(2,128)(2,1)} %bitcast.20), calls=%async_computation.4 | async-start | bytes 262144 | tf_op jit(solution)/shard_map/all_to_all | solution.py:154
  83.0 6.9 %copy-start.6 = (bf16[2048,32]{0,1:T(8,128)(2,1)S(1)}, bf16[2048,32]{0,1:T(8,128)(2,1)}, u32[]{:S(2)}) copy-start(bf16[2048,32]{0,1:T(8,128)(2,1)} %param.41) | copy-start | bytes 393220
  86.3 10.3 %all-to-all-start.5 = ((bf16[16,1,2,2048]{3,2,1,0:T(2,128)(2,1)}), bf16[16,1,2,2048]{3,2,1,0:T(2,128)(2,1)S(1)}, u32[]{:S(2)}, u32[]{:S(2)}) async-start(bf16[16,1,2,2048]{3,2,1,0:T(2,128)(2,1)} %copy.77), calls=%async_computation.5 | async-start | bytes 262144 | tf_op jit(solution)/shard_map/all_to_all | solution.py:159
  100.9 2.3 %copy-start.4 = (bf16[32,2048]{1,0:T(8,128)(2,1)S(1)}, bf16[32,2048]{1,0:T(8,128)(2,1)}, u32[]{:S(2)}) copy-start(bf16[32,2048]{1,0:T(8,128)(2,1)} %param.43) | copy-start | bytes 393220
  100.9 2.3 %copy-start.5 = (bf16[2048,32]{0,1:T(8,128)(2,1)S(1)}, bf16[2048,32]{0,1:T(8,128)(2,1)}, u32[]{:S(2)}) copy-start(bf16[2048,32]{0,1:T(8,128)(2,1)} %param.42) | copy-start | bytes 393220
  104.3 14.5 %all-to-all-start.6 = ((bf16[16,32,128]{2,1,0:T(8,128)(2,1)}), bf16[16,32,128]{2,1,0:T(8,128)(2,1)S(1)}, u32[]{:S(2)}, u32[]{:S(2)}) async-start(bf16[16,32,128]{2,1,0:T(8,128)(2,1)} %bitcast.219), calls=%async_computation.6 | async-start | bytes 262144 | tf_op jit(solution)/shard_map/all_to_all | solution.py:34
where the time goes:
time: 120 us; the launch traced here: 119 us
  waiting for transfers between devices  48.7 us (41%)
  starting transfers between devices  36.3 us (30%)
  matrix products  13.2 us (11%)
  local copies, waits for them, and re-layouts  9.73 us (8%)
  other arithmetic  9.18 us (8%)
  between operations  2.25 us (2%)
    all_to_all x3, waiting for transfers between devices, copy_for_each(): lax.all_to_all(jnp.broadcast_to(array[None], (length, *array.shape)), axi...  19.9 us
    all_to_all x3, starting transfers between devices, copy_for_each(): lax.all_to_all(jnp.broadcast_to(array[None], (length, *array.shape)), axi...  17.3 us
    all_to_all x2, waiting for transfers between devices, summed_on_arrival(): lax.all_to_all(parts, axis, split_axis=0, concat_axis=0, tiled=True)  14.9 us
    all_to_all x2, starting transfers between devices, summed_on_arrival(): lax.all_to_all(parts, axis, split_axis=0, concat_axis=0, tiled=True)  8.76 us
    all_to_all x1, waiting for transfers between devices, body(): lax.all_to_all(outgoing, 'ep', split_axis=0, concat_axis=0, tiled=True)  7.32 us
    all_to_all x1, starting transfers between devices, body(): lax.all_to_all(outgoing, 'ep', split_axis=0, concat_axis=0, tiled=True)  6.76 us
    all_to_all x1, waiting for transfers between devices, body(): lax.all_to_all(results, 'ep', split_axis=0, concat_axis=0, tiled=True)  6.64 us
    dot_general x4, matrix products, project(): result = jnp.dot(normed_mix, weight, preferred_element_type=jnp.float32)  4.29 us
  transfers between devices with their start and end apart: 7, of which 7 were waited for; matrix products, arithmetic and copies ran while one was open for 6% of the time, Pallas kernels for 0%

commit v1 on v0

v1 whole, which is shorter than its diff:
```python
import jax
import jax.numpy as jnp
from jax import lax
from jax.experimental import pallas as pl
from jax.experimental.pallas import tpu as pltpu
from jax.sharding import PartitionSpec as P

EPS = 1e-06
MESH = pl.DeviceIdType.MESH
BF = jnp.bfloat16
F32 = jnp.float32
NT = (((1,), (1,)), ((), ()))


def silu(v):
    return v * jax.nn.sigmoid(v)


def dot(a, b):
    return jnp.dot(a, b, preferred_element_type=F32)


def dot_nt(a, b):
    return lax.dot_general(a, b, NT, preferred_element_type=F32)


def row(ref):
    return ref[...].astype(F32).reshape(1, -1)


def kernel(
    tokens, state, mix_gain, w_query, w_key, w_value, w_outgate, w_beta, w_decay, decay_scale, decay_bias,
    head_gain, w_output, ffn_gain, ids, weights, e_gate, e_up, e_down, s_gate, s_up, s_down,
    out, new_state,
    tok_all, st, proj_w, wb, wd, dscale, dbias, mgain, hgain, wo, fgain, idv, rwv, eg, eu, ed, sg, su, sd,
    mix_send, mix_recv, disp_send, disp_recv, res_all, back_send, back_recv, sh_send, sh_recv,
    onehot, comb, k_read, q_read, out_v,
    local_sem, send_sem, recv_sem, entered,
):
    n_ep, n_tp = 16, 16
    ep, tp = lax.axis_index("ep"), lax.axis_index("tp")
    me = ep * n_tp + tp
    rows, width = tokens.shape
    dk = state.shape[2]
    top = ids.shape[0]

    barrier = pltpu.get_barrier_semaphore()
    for d in range(1, n_tp):
        pl.semaphore_signal(barrier, inc=1, device_id=(ep, lax.rem(tp + d, n_tp)), device_id_type=MESH)
        pl.semaphore_signal(barrier, inc=1, device_id=(lax.rem(ep + d, n_ep), tp), device_id_type=MESH)

    fetches = []

    def fetch(src, dst):
        copy = pltpu.make_async_copy(src, dst, local_sem.at[len(fetches)])
        fetches.append(copy)
        copy.start()
        return copy

    c_tok = fetch(tokens, tok_all.at[tp])
    c_route = [fetch(ids, idv), fetch(weights, rwv)]
    c_mix = [
        fetch(mix_gain, mgain), fetch(w_beta, wb), fetch(w_decay, wd), fetch(decay_scale, dscale),
        fetch(decay_bias, dbias), fetch(head_gain, hgain), fetch(ffn_gain, fgain),
    ]
    for i, w in enumerate((w_query, w_key, w_value, w_outgate)):
        c_mix.append(fetch(w, proj_w.at[:, pl.ds(i * dk, dk)]))
    c_mix.append(fetch(state.at[:, 0], st))
    c_mix.append(fetch(w_output, wo))
    c_sh = [fetch(s_gate, sg), fetch(s_up, su), fetch(s_down, sd)]
    c_ex = [fetch(e_gate.at[0], eg), fetch(e_up.at[0], eu), fetch(e_down.at[0], ed)]

    def total(ref, count, sem):
        return pltpu.make_async_copy(ref.at[pl.ds(0, count)], ref.at[pl.ds(0, count)], sem)

    def to_row(src, dst, phase, d):
        pltpu.make_async_remote_copy(
            src, dst, send_sem.at[phase], recv_sem.at[phase],
            device_id=(ep, lax.rem(tp + d, n_tp)), device_id_type=MESH,
        ).start()

    far_first = [8, 9, 7, 10, 6, 11, 5, 12, 4, 13, 3, 14, 2, 15, 1]

    c_tok.wait()
    pl.semaphore_wait(barrier, n_ep + n_tp - 2)
    for d in far_first:
        to_row(tok_all.at[tp], tok_all.at[tp], 0, d)
    for d in range(1, n_ep):
        pl.semaphore_signal(entered, inc=1, device_id=(lax.rem(ep + d, n_ep), tp), device_id_type=MESH)

    for c in c_route:
        c.wait()
    slots = 2 * n_ep * n_tp
    lower = (lax.broadcasted_iota(jnp.int32, (rows, rows), 0) < lax.broadcasted_iota(jnp.int32, (rows, rows), 1)).astype(BF)

    def placed(slot):
        expert, seat = slot // 2, lax.rem(slot, 2)
        named = jnp.zeros(slot.shape, F32)
        weight = jnp.zeros(slot.shape, F32)
        for j in range(top):
            hit = idv[j : j + 1, :] == expert
            named = jnp.where(hit, 1.0, named)
            weight = jnp.where(hit, rwv[j : j + 1, :], weight)
        before = dot(named.astype(BF), lower)
        here = (named > 0.5) & (before == seat.astype(F32))
        return here, weight

    here, weight = placed(lax.broadcasted_iota(jnp.int32, (slots, rows), 0))
    onehot[...] = jnp.where(here, 1.0, 0.0).astype(BF)
    weight = jnp.where(here, weight, 0.0).T
    high = weight.astype(BF)
    comb[0:rows, :] = high
    comb[rows : 2 * rows, :] = (weight - high.astype(F32)).astype(BF)
    pair_row = lax.broadcasted_iota(jnp.int32, (rows, rows), 0)
    own_pair = pair_row // 2 == ep
    own_here, own_weight = placed(2 * me + lax.rem(pair_row, 2))
    own_here = own_here & own_pair
    own_onehot = jnp.where(own_here, 1.0, 0.0).astype(BF)
    own_weight = jnp.where(own_here, own_weight, 0.0).T
    own_high = own_weight.astype(BF)
    own_comb = jnp.concatenate([own_high, (own_weight - own_high.astype(F32)).astype(BF)], axis=0)

    for c in c_mix:
        c.wait()
    total(tok_all, n_tp - 1, recv_sem.at[0]).wait()

    def normed_rows(blocks, gain_row):
        values = jnp.concatenate(blocks, axis=1).astype(F32)
        squares = jnp.mean(values * values, axis=1, keepdims=True)
        return (values * lax.rsqrt(squares + EPS) * gain_row).astype(BF)

    normed = normed_rows([tok_all[t] for t in range(n_tp)], row(mgain))
    projected = dot(normed, proj_w[...]).astype(BF).astype(F32)
    query, key, value, gate = (projected[:, i * dk : (i + 1) * dk] for i in range(4))

    def unit(v):
        return v * lax.rsqrt(jnp.sum(v * v, axis=1, keepdims=True) + EPS)

    query = unit(query) * dk ** (-0.5)
    key = unit(key)
    wide = normed.astype(F32)
    beta = jax.nn.sigmoid(jnp.sum(wide * wb[...].astype(F32), axis=1, keepdims=True))
    decay_in = jnp.sum(wide * wd[...].astype(F32), axis=1, keepdims=True) + dbias[0]
    softplus = jnp.maximum(decay_in, 0.0) + jnp.log(1.0 + jnp.exp(-jnp.abs(decay_in)))
    decay = jnp.exp(-dscale[0] * softplus)
    key_t, query_t = key.T, query.T
    for s in range(rows):
        block = st[s]
        k_read[s : s + 1, :] = jnp.sum(block * key_t[:, s : s + 1], axis=0, keepdims=True)
        q_read[s : s + 1, :] = jnp.sum(block * query_t[:, s : s + 1], axis=0, keepdims=True)
    written = beta * (value - decay * k_read[...])
    read = decay * q_read[...] + jnp.sum(query * key, axis=1, keepdims=True) * written
    squares = jnp.mean(read * read, axis=1, keepdims=True)
    gated = (read * lax.rsqrt(squares + EPS) * row(hgain) * silu(gate)).astype(BF)
    partial = dot(gated, wo[...])
    own_partial = jnp.zeros((rows, width), F32)
    for t in range(n_tp):
        piece = partial[:, t * width : (t + 1) * width]
        mix_send[t] = piece.astype(BF)
        own_partial = jnp.where(tp == t, piece, own_partial)
    for d in far_first:
        to_row(mix_send.at[lax.rem(tp + d, n_tp)], mix_recv.at[d - 1], 1, d)

    for s in range(rows):
        st[s] = decay[s : s + 1, :] * st[s] + key_t[:, s : s + 1] * written[s : s + 1, :]
    c_state = pltpu.make_async_copy(st, new_state.at[:, 0], local_sem.at[len(fetches)])
    c_state.start()

    total(mix_recv, n_tp - 1, recv_sem.at[1]).wait()
    mixed = own_partial
    for d in range(n_tp - 1):
        mixed = mixed + mix_recv[d].astype(F32)
    resid = tok_all[tp].astype(F32) + mixed
    resid_b = resid.astype(BF)

    disp_send[...] = dot(onehot[...], resid_b).astype(BF)
    res_all[tp] = resid_b
    pl.semaphore_wait(entered, n_ep - 1)

    @pl.loop(1, n_ep * n_tp, unroll=5)
    def _(d):
        peer = lax.rem(me + d, n_ep * n_tp)
        pltpu.make_async_remote_copy(
            disp_send.at[pl.ds(pl.multiple_of(2 * peer, 2), 2)],
            disp_recv.at[tp, pl.ds(pl.multiple_of(2 * ep, 2), 2)],
            send_sem.at[2], recv_sem.at[2],
            device_id=(peer // n_tp, lax.rem(peer, n_tp)), device_id_type=MESH,
        ).start()

    for d in far_first:
        to_row(res_all.at[tp], res_all.at[tp], 3, d)
    own_disp = dot(own_onehot, resid_b).astype(BF)

    for c in c_ex:
        c.wait()
    pltpu.make_async_copy(back_recv.at[pl.ds(0, slots - 2)], back_recv.at[pl.ds(0, slots - 2)], recv_sem.at[2]).wait()
    fgain_row = row(fgain)
    own_block = lax.broadcasted_iota(jnp.int32, (rows, width), 0) // 2 == ep
    routed_rows = normed_rows(
        [jnp.where(own_block & (tp == t), own_disp, disp_recv[t]) for t in range(n_tp)], fgain_row
    )
    hidden = (silu(dot(routed_rows, eg[...])) * dot(routed_rows, eu[...])).astype(BF)
    results = dot(hidden, ed[...])
    own_back = jnp.zeros((rows, width), F32)
    for t in range(n_tp):
        piece = results[:, t * width : (t + 1) * width]
        back_send[t] = piece.astype(BF)
        own_back = jnp.where(tp == t, piece, own_back)

    @pl.loop(1, n_ep * n_tp, unroll=5)
    def _(d):
        peer = lax.rem(me + d, n_ep * n_tp)
        to_ep, to_tp = peer // n_tp, lax.rem(peer, n_tp)
        pltpu.make_async_remote_copy(
            back_send.at[to_tp, pl.ds(pl.multiple_of(2 * to_ep, 2), 2)],
            back_recv.at[pl.ds(pl.multiple_of(2 * me, 2), 2)],
            send_sem.at[4], recv_sem.at[4],
            device_id=(to_ep, to_tp), device_id_type=MESH,
        ).start()

    for c in c_sh:
        c.wait()
    total(res_all, n_tp - 1, recv_sem.at[3]).wait()
    normed_ffn = normed_rows([res_all[t] for t in range(n_tp)], fgain_row)
    hidden_shared = (silu(dot_nt(normed_ffn, sg[...])) * dot_nt(normed_ffn, su[...])).astype(BF)
    shared = dot(hidden_shared, sd[...])
    own_shared = jnp.zeros((rows, width), F32)
    for t in range(n_tp):
        piece = shared[:, t * width : (t + 1) * width]
        sh_send[t] = piece.astype(BF)
        own_shared = jnp.where(tp == t, piece, own_shared)
    for d in far_first:
        to_row(sh_send.at[lax.rem(tp + d, n_tp)], sh_recv.at[d - 1], 5, d)

    own_routed = dot(own_comb, own_back.astype(BF))
    final = resid + own_shared + own_routed[0:rows] + own_routed[rows : 2 * rows]
    total(sh_recv, n_tp - 1, recv_sem.at[5]).wait()
    for d in range(n_tp - 1):
        final = final + sh_recv[d].astype(F32)
    pltpu.make_async_copy(back_recv.at[pl.ds(0, slots - 2)], back_recv.at[pl.ds(0, slots - 2)], recv_sem.at[4]).wait()
    own_rows = lax.broadcasted_iota(jnp.int32, (slots, width), 0) // 2 == me
    arrived = jnp.where(own_rows, jnp.zeros((slots, width), BF), back_recv[...])
    routed = dot(comb[...], arrived)
    out_v[...] = (final + routed[0:rows] + routed[rows : 2 * rows]).astype(BF)
    c_out = pltpu.make_async_copy(out_v, out, local_sem.at[len(fetches) + 1])
    c_out.start()

    for phase, ref in ((0, tok_all), (1, mix_recv), (3, res_all), (5, sh_recv)):
        total(ref, n_tp - 1, send_sem.at[phase]).wait()
    for phase in (2, 4):
        pltpu.make_async_copy(
            back_recv.at[pl.ds(0, slots - 2)], back_recv.at[pl.ds(0, slots - 2)], send_sem.at[phase]
        ).wait()
    c_state.wait()
    c_out.wait()


def body(
    tokens, delta_state, mix_gain, w_query, w_key, w_value, w_outgate, w_beta, w_decay, decay_scale, decay_bias,
    head_gain, w_output, ffn_gain, route_ids, route_weights, expert_gate, expert_up, expert_down, shared_gate,
    shared_up, shared_down,
):
    rows, width = tokens.shape
    n_ep, n_tp = lax.axis_size("ep"), lax.axis_size("tp")
    model, dk = w_query.shape
    top = route_ids.shape[1]
    fe = expert_gate.shape[2]
    fs = shared_gate.shape[1]
    slots = 2 * n_ep * n_tp
    block = (n_tp, rows, width)
    V = pltpu.VMEM
    dma = pltpu.SemaphoreType.DMA
    return pl.pallas_call(
        kernel,
        out_shape=(
            jax.ShapeDtypeStruct(tokens.shape, tokens.dtype),
            jax.ShapeDtypeStruct(delta_state.shape, delta_state.dtype),
        ),
        in_specs=[pl.BlockSpec(memory_space=pl.ANY)] * 22,
        out_specs=(pl.BlockSpec(memory_space=pl.ANY),) * 2,
        scratch_shapes=[
            V(block, BF),
            V((rows, dk, dk), F32),
            V((model, 4 * dk), BF),
            V((1, model), BF),
            V((1, model), BF),
            pltpu.SMEM((1,), F32),
            pltpu.SMEM((1,), F32),
            V((model,), BF),
            V((dk,), BF),
            V((dk, model), BF),
            V((model,), BF),
            V((top, rows), jnp.int32),
            V((top, rows), F32),
            V((model, fe), BF),
            V((model, fe), BF),
            V((fe, model), BF),
            V((fs, model), BF),
            V((fs, model), BF),
            V((fs, model), BF),
            V(block, BF),
            V((n_tp - 1, rows, width), BF),
            V((slots, width), BF),
            V(block, BF),
            V(block, BF),
            V(block, BF),
            V((slots, width), BF),
            V(block, BF),
            V((n_tp - 1, rows, width), BF),
            V((slots, rows), BF),
            V((2 * rows, slots), BF),
            V((rows, dk), F32),
            V((rows, dk), F32),
            V((rows, width), BF),
            dma((24,)),
            dma((6,)),
            dma((6,)),
            pltpu.SemaphoreType.REGULAR,
        ],
        compiler_params=pltpu.CompilerParams(collective_id=0, has_side_effects=True),
        name="layer",
    )(
        tokens, delta_state, mix_gain, w_query, w_key, w_value, w_outgate, w_beta.T, w_decay.T, decay_scale,
        decay_bias, head_gain, w_output, ffn_gain, route_ids.T, route_weights.T, expert_gate, expert_up, expert_down,
        shared_gate.T, shared_up.T, shared_down,
    )


def solution(mesh):
    return jax.shard_map(
        body,
        mesh=mesh,
        in_specs=(
            P("ep", "tp"),
            P("ep", "tp", None, None),
            P(),
            P(None, "tp"),
            P(None, "tp"),
            P(None, "tp"),
            P(None, "tp"),
            P(None, "tp"),
            P(None, "tp"),
            P("tp"),
            P("tp"),
            P(),
            P("tp", None),
            P(),
            P("ep", None),
            P("ep", None),
            P(("ep", "tp"), None, None),
            P(("ep", "tp"), None, None),
            P(("ep", "tp"), None, None),
            P(None, "tp"),
            P(None, "tp"),
            P("tp", None),
        ),
        out_specs=(P("ep", "tp"), P("ep", "tp", None, None)),
        check_vma=False,
    )
```

time: 120 us -> 51.9 us (0.43)
  waiting for transfers between devices: 48.7 us -> 0 us
  Pallas kernels: 0 us -> 45.3 us
  starting transfers between devices: 36.3 us -> 0 us
  matrix products: 13.2 us -> 0 us
  other arithmetic: 9.18 us -> 0 us
  local copies, waits for them, and re-layouts: 9.73 us -> 4.43 us
    all_to_all x7 -> x0, waiting for transfers between devices: 48.7 us -> none  [the longest x3 19.9 us: copy_for_each(): lax.all_to_all(jnp.broadcast_to(array[None], (length, *array.shape)), axi...]
    pallas_call x0 -> x1, Pallas kernels: none -> 45.3 us  [body(): pl.pallas_call(kernel, out_shape=(jax.ShapeDtypeStruct(tokens.shape, toke...]
    all_to_all x7 -> x0, starting transfers between devices: 36.3 us -> none  [the longest x3 17.3 us: copy_for_each(): lax.all_to_all(jnp.broadcast_to(array[None], (length, *array.shape)), axi...]
    dot_general x15 -> x0, matrix products: 13.2 us -> none  [the longest x4 4.29 us: project(): result = jnp.dot(normed_mix, weight, preferred_element_type=jnp.float32)]
    reshape x7 -> x0, local copies, waits for them, and re-layouts: 5.01 us -> none  [the longest x1 2.65 us: body(): (pair_weights[:, None] * picked).reshape(rows_count, top_count, model_width)]
    unnamed x24 -> x2, local copies, waits for them, and re-layouts: 0.92 us -> 4.43 us
    reduce_sum x11 -> x0, other arithmetic: 3.2 us -> none  [the longest x1 2.27 us: body(): jnp.sum((pair_weights[:, None] * picked).reshape(rows_count, top_count, m...]
    add x1 -> x0, other arithmetic: 2.94 us -> none  [body(): decay_rate[:, :, None, None] * kept_state]
  transfers between devices with their start and end apart: 7 -> 0, of which waited for: 7 -> 0; matrix products, arithmetic and copies ran while one was open for 6% -> 0% of each run, Pallas kernels for 0% -> 0%
where the time goes in v1:
time: 51.9 us; the launch traced here: 51.7 us
  Pallas kernels  45.3 us (87%)
  local copies, waits for them, and re-layouts  4.43 us (9%)
  between operations  1.94 us (4%)
    pallas_call x1, Pallas kernels, body(): pl.pallas_call(kernel, out_shape=(jax.ShapeDtypeStruct(tokens.shape, toke...  45.3 us
    unnamed x2, local copies, waits for them, and re-layouts  4.43 us

profile of v1, /device:TPU:1, one launch (start us, length us, event | category | flops | bytes accessed | tf_op | source)
XLA Modules:
  0.0 51.7 jit_solution(11792607034611260213)
XLA Ops:
  1.9 45.3 %layer.1 = (bf16[32,128]{1,0:T(8,128)(2,1)}, f32[32,1,128,128]{3,2,1,0:T(8,128)}) custom-call(bf16[32,128]{1,0:T(8,128)(2,1)} %tokens.1, f32[32,1,128,128]{3,2,1,0:T(8,128)} %state.1, bf16[2048]{0:T(1024)(128)(2,1)} %mix_gain.1, bf16[2048,128]{1,0:T(8,128)(2,1)} %w_query.1, bf16[2048,128]{1,0:T(8,128)(2,1)} %w_key.1, bf16[2048,128]{1,0:T(8,128)(2,1)} %w_value.1, ...), custom_call_target="tpu_custom_call" | custom-call | tf_op jit(solution)/shard_map/layer/pallas_call | solution.py:273
  47.3 1.3 %copy.28 = bf16[32,128]{1,0:T(8,128)(2,1)} copy(bf16[32,128]{1,0:T(8,128)(2,1)} %get-tuple-element.4) | data formatting | bytes 16384
  48.6 3.1 %copy.29 = f32[32,1,128,128]{3,2,1,0:T(8,128)} copy(f32[32,1,128,128]{3,2,1,0:T(8,128)} %get-tuple-element.5) | data formatting | bytes 4194304

commit v2 on v1

v2 whole, which is shorter than its diff:
```python
import jax
import jax.numpy as jnp
from jax import lax
from jax.experimental import pallas as pl
from jax.experimental.pallas import tpu as pltpu
from jax.sharding import PartitionSpec as P

EPS = 1e-06
MESH = pl.DeviceIdType.MESH
BF = jnp.bfloat16
F32 = jnp.float32
NT = (((1,), (1,)), ((), ()))


def silu(v):
    return v * jax.nn.sigmoid(v)


def dot(a, b):
    return jnp.dot(a, b, preferred_element_type=F32)


def dot_nt(a, b):
    return lax.dot_general(a, b, NT, preferred_element_type=F32)


def row(ref):
    return ref[...].astype(F32).reshape(1, -1)


ZO = (4, 3, 5, 2, 6, 1, 7, 0)
RO = (2, 1, 3, 0)


def ring(i, n):
    half = i // 2
    return n // 2 + half - lax.rem(i, 2) * (2 * half + 1)


def kernel(
    tokens, state, mix_gain, w_query, w_key, w_value, w_outgate, w_beta, w_decay, decay_scale, decay_bias,
    head_gain, w_output, ffn_gain, ids, weights, e_gate, e_up, e_down, s_gate, s_up, s_down,
    out, st,
    tok_all, st_split, proj_w, wb, wd, dscale, dbias, mgain, hgain, wo, fgain, fgain8, idv, rwv, eg, eu, ed, sg, su, sd,
    mix_send, mix_recv, disp_send, disp_recv, res_all, back_send, back_recv, sh_send, sh_recv,
    onehot, comb, k_read, q_read, sized,
    local_sem, send_sem, recv_sem, entered,
):
    n_ep, n_tp = 16, 16
    ep, tp = lax.axis_index("ep"), lax.axis_index("tp")
    me = ep * n_tp + tp
    y, x = ep // 4, lax.rem(ep, 4)
    z, core = tp // 2, lax.rem(tp, 2)
    rows, width = tokens.shape
    dk = state.shape[2]
    top = ids.shape[0]
    slots = 2 * n_ep * n_tp
    wide2 = 2 * width

    barrier = pltpu.get_barrier_semaphore()
    for d in range(1, n_tp):
        pl.semaphore_signal(barrier, inc=1, device_id=(ep, lax.rem(tp + d, n_tp)), device_id_type=MESH)
        pl.semaphore_signal(barrier, inc=1, device_id=(lax.rem(ep + d, n_ep), tp), device_id_type=MESH)

    fetches = []

    def fetch(src, dst):
        copy = pltpu.make_async_copy(src, dst, local_sem.at[len(fetches)])
        fetches.append(copy)
        copy.start()
        return copy

    c_tok = fetch(tokens, tok_all.at[tp])
    c_route = [fetch(ids, idv), fetch(weights, rwv)]
    c_state = fetch(state.at[:, 0], st)
    c_mix = [
        fetch(mix_gain, mgain), fetch(w_beta, wb), fetch(w_decay, wd), fetch(decay_scale, dscale),
        fetch(decay_bias, dbias), fetch(head_gain, hgain), fetch(ffn_gain, fgain),
    ]
    for i, w in enumerate((w_query, w_key, w_value, w_outgate)):
        c_mix.append(fetch(w, proj_w.at[:, pl.ds(i * dk, dk)]))
    c_mix.append(fetch(w_output, wo))
    c_sh = [fetch(s_gate, sg), fetch(s_up, su), fetch(s_down, sd)]
    c_ex = []
    z_from = [lax.rem(z + 8 - ZO[a], 8) for a in range(8)]
    z_to = [lax.rem(z + ZO[a], 8) for a in range(8)]
    for a in range(8):
        here, there = pl.ds(a * wide2, wide2), pl.ds(pl.multiple_of(z_from[a] * wide2, wide2), wide2)
        c_ex += [fetch(e_gate.at[0, there], eg.at[here]), fetch(e_up.at[0, there], eu.at[here])]
        there = pl.ds(pl.multiple_of(z_to[a] * wide2, wide2), wide2)
        c_ex.append(fetch(e_down.at[0, :, there], ed.at[:, here]))

    def total(ref, count, sem):
        return pltpu.make_async_copy(ref.at[pl.ds(0, count)], ref.at[pl.ds(0, count)], sem)

    def to_row(src, dst, phase, d):
        pltpu.make_async_remote_copy(
            src, dst, send_sem.at[phase], recv_sem.at[phase],
            device_id=(ep, lax.rem(tp + d, n_tp)), device_id_type=MESH,
        ).start()

    far_first = [8, 9, 7, 10, 6, 11, 5, 12, 4, 13, 3, 14, 2, 15, 1]

    c_tok.wait()
    pl.semaphore_wait(barrier, n_ep + n_tp - 2)
    for d in far_first:
        to_row(tok_all.at[tp], tok_all.at[tp], 0, d)
    for d in range(1, n_ep):
        pl.semaphore_signal(entered, inc=1, device_id=(lax.rem(ep + d, n_ep), tp), device_id_type=MESH)

    for c in c_route:
        c.wait()
    lower = (
        lax.broadcasted_iota(jnp.int32, (rows, rows), 0) < lax.broadcasted_iota(jnp.int32, (rows, rows), 1)
    ).astype(BF)

    def placed(expert, seat):
        named = jnp.zeros(expert.shape, F32)
        weight = jnp.zeros(expert.shape, F32)
        for j in range(top):
            hit = idv[j : j + 1, :] == expert
            named = jnp.where(hit, 1.0, named)
            weight = jnp.where(hit, rwv[j : j + 1, :], weight)
        before = dot(named.astype(BF), lower)
        return (named > 0.5) & (before == seat.astype(F32)), weight

    slot = lax.broadcasted_iota(jnp.int32, (slots, rows), 0)
    pair = slot // 2
    seat = slot - 2 * pair
    off_x, off_y = ring(pair % 4, 4), ring((pair // 4) % 4, 4)
    off_z, slot_core = ring(pair // 32, 8), (pair // 16) % 2
    far_ep = ((y + off_y) % 4) * 4 + (x + off_x) % 4
    here, _ = placed(far_ep * n_tp + ((z + off_z) % 8) * 2 + slot_core, seat)
    onehot[...] = jnp.where(here, 1.0, 0.0).astype(BF)
    here, weight = placed(far_ep * n_tp + ((z + 8 - off_z) % 8) * 2 + slot_core, seat)
    weight = jnp.where(here, weight, 0.0).T
    high = weight.astype(BF)
    comb[0:rows, :] = high
    comb[rows : 2 * rows, :] = (weight - high.astype(F32)).astype(BF)
    pair_row = lax.broadcasted_iota(jnp.int32, (rows, rows), 0)
    own_here, own_weight = placed(jnp.full((rows, rows), 0, jnp.int32) + me, pair_row % 2)
    own_here = own_here & (pair_row // 2 == n_ep - 1)
    own_onehot = jnp.where(own_here, 1.0, 0.0).astype(BF)
    own_weight = jnp.where(own_here, own_weight, 0.0).T
    own_high = own_weight.astype(BF)
    own_comb = jnp.concatenate([own_high, (own_weight - own_high.astype(F32)).astype(BF)], axis=0)

    c_state.wait()

    @pl.loop(0, rows, unroll=4)
    def _(s):
        block = st[s]
        high = block.astype(BF)
        st_split[s, 0:dk, :] = high
        st_split[s, dk : 2 * dk, :] = (block - high.astype(F32)).astype(BF)

    for c in c_mix:
        c.wait()
    fgain_row = row(fgain)
    for i in range(8):
        fgain8[i : i + 1, :] = fgain_row[:, i * wide2 : (i + 1) * wide2]
    total(tok_all, n_tp - 1, recv_sem.at[0]).wait()

    def normed_rows(blocks, gain_row):
        values = jnp.concatenate(blocks, axis=1).astype(F32)
        squares = jnp.mean(values * values, axis=1, keepdims=True)
        return (values * lax.rsqrt(squares + EPS) * gain_row).astype(BF)

    normed = normed_rows([tok_all[t] for t in range(n_tp)], row(mgain))
    projected = dot(normed, proj_w[...]).astype(BF).astype(F32)
    query, key, value, gate = (projected[:, i * dk : (i + 1) * dk] for i in range(4))

    def unit(v):
        return v * lax.rsqrt(jnp.sum(v * v, axis=1, keepdims=True) + EPS)

    query = unit(query) * dk ** (-0.5)
    key = unit(key)

    def two_parts(v):
        high = v.astype(BF).astype(F32)
        return high, v - high

    k_high, k_low = two_parts(key)
    q_high, q_low = two_parts(query)
    for s0 in range(0, rows, 8):
        some = slice(s0, s0 + 8)
        left = jnp.concatenate([k_high[some], q_high[some], k_low[some], q_low[some]], axis=0).astype(BF)
        left = jnp.concatenate([left, left], axis=1)
        for i in range(8):
            s = s0 + i
            both = dot(left, st_split[s])
            k_read[s : s + 1, :] = both[i : i + 1] + both[16 + i : 17 + i]
            q_read[s : s + 1, :] = both[8 + i : 9 + i] + both[24 + i : 25 + i]
    wide = normed.astype(F32)
    beta = jax.nn.sigmoid(jnp.sum(wide * wb[...].astype(F32), axis=1, keepdims=True))
    decay_in = jnp.sum(wide * wd[...].astype(F32), axis=1, keepdims=True) + dbias[0]
    softplus = jnp.maximum(decay_in, 0.0) + jnp.log(1.0 + jnp.exp(-jnp.abs(decay_in)))
    decay = jnp.exp(-dscale[0] * softplus)
    written = beta * (value - decay * k_read[...])
    read = decay * q_read[...] + jnp.sum(query * key, axis=1, keepdims=True) * written
    squares = jnp.mean(read * read, axis=1, keepdims=True)
    gated = (read * lax.rsqrt(squares + EPS) * row(hgain) * silu(gate)).astype(BF)
    partial = dot(gated, wo[...])
    own_partial = jnp.zeros((rows, width), F32)
    for t in range(n_tp):
        piece = partial[:, t * width : (t + 1) * width]
        mix_send[t] = piece.astype(BF)
        own_partial = jnp.where(tp == t, piece, own_partial)
    for d in far_first:
        to_row(mix_send.at[lax.rem(tp + d, n_tp)], mix_recv.at[d - 1], 1, d)

    key_t = key.T
    for s in range(rows):
        st[s] = decay[s : s + 1, :] * st[s] + key_t[:, s : s + 1] * written[s : s + 1, :]

    total(mix_recv, n_tp - 1, recv_sem.at[1]).wait()
    mixed = own_partial
    for d in range(n_tp - 1):
        mixed = mixed + mix_recv[d].astype(F32)
    resid = tok_all[tp].astype(F32) + mixed
    resid_b = resid.astype(BF)

    res_all[tp] = resid_b
    disp_send[...] = dot(onehot[...], resid_b).astype(BF).reshape(disp_send.shape)

    def to_all(src, dst, phase, sign):
        to_y = [lax.rem(y + 4 + sign * r, 4) * 4 for r in RO]
        to_x = [lax.rem(x + 4 + sign * r, 4) for r in RO]
        to_ep = [to_y[b] + to_x[e] for b in range(4) for e in range(4)]

        def send(a, c, i, dev_tp):
            seats = pl.ds(2 * i, 2)
            pltpu.make_async_remote_copy(
                src.at[a, c, seats], dst.at[a, core, seats], send_sem.at[phase], recv_sem.at[phase],
                device_id=(to_ep[i], dev_tp), device_id_type=MESH,
            ).start()

        @pl.loop(0, 7)
        def _(a):
            dev_tp = lax.rem(z + ring(a, 8), 8) * 2
            for i in range(16):
                for c in range(2):
                    send(a, c, i, dev_tp + c)

        for i in range(15):
            for c in range(2):
                send(7, c, i, 2 * z + c)
        send(7, 1 - core, 15, 2 * z + 1 - core)

    def all_sent(sem):
        as_many = sized.at[pl.ds(0, slots - 2)]
        return pltpu.make_async_copy(as_many, as_many, sem)

    pl.semaphore_wait(entered, n_ep - 1)
    to_all(disp_send, disp_recv, 2, 1)
    for d in far_first:
        to_row(res_all.at[tp], res_all.at[tp], 3, d)
    own_disp = dot(own_onehot, resid_b).astype(BF)

    for c in c_ex:
        c.wait()
    all_sent(recv_sem.at[2]).wait()
    own_block = lax.broadcasted_iota(jnp.int32, (rows, width), 0) // 2 == n_ep - 1
    blocks = [disp_recv[a, c] for a in range(8) for c in range(2)]
    for c in range(2):
        blocks[14 + c] = jnp.where(own_block & (core == c), own_disp, blocks[14 + c])
    gain_from = jnp.concatenate([fgain8[pl.ds(z_from[a], 1), :] for a in range(8)], axis=1)
    routed_rows = normed_rows(blocks, gain_from)
    hidden = (silu(dot(routed_rows, eg[...])) * dot(routed_rows, eu[...])).astype(BF)
    results = dot(hidden, ed[...])
    for a in range(8):
        for c in range(2):
            back_send[a, c] = results[:, (2 * a + c) * width : (2 * a + c + 1) * width].astype(BF)
    own_back = jnp.where(core == 0, results[:, 14 * width : 15 * width], results[:, 15 * width : 16 * width])
    to_all(back_send, back_recv, 4, -1)

    for c in c_sh:
        c.wait()
    total(res_all, n_tp - 1, recv_sem.at[3]).wait()
    normed_ffn = normed_rows([res_all[t] for t in range(n_tp)], fgain_row)
    hidden_shared = (silu(dot_nt(normed_ffn, sg[...])) * dot_nt(normed_ffn, su[...])).astype(BF)
    shared = dot(hidden_shared, sd[...])
    own_shared = jnp.zeros((rows, width), F32)
    for t in range(n_tp):
        piece = shared[:, t * width : (t + 1) * width]
        sh_send[t] = piece.astype(BF)
        own_shared = jnp.where(tp == t, piece, own_shared)
    for d in far_first:
        to_row(sh_send.at[lax.rem(tp + d, n_tp)], sh_recv.at[d - 1], 5, d)
    own_routed = dot(own_comb, own_back.astype(BF))
    final = resid + own_shared + own_routed[0:rows] + own_routed[rows : 2 * rows]
    total(sh_recv, n_tp - 1, recv_sem.at[5]).wait()
    for d in range(n_tp - 1):
        final = final + sh_recv[d].astype(F32)
    all_sent(recv_sem.at[4]).wait()
    own_rows = lax.broadcasted_iota(jnp.int32, (slots, width), 0) // 2 == (14 + core) * n_ep + n_ep - 1
    arrived = jnp.where(own_rows, jnp.zeros((slots, width), BF), back_recv[...].reshape(slots, width))
    routed = dot(comb[...], arrived)
    out[...] = (final + routed[0:rows] + routed[rows : 2 * rows]).astype(BF)

    for phase, ref in ((0, tok_all), (1, mix_recv), (3, res_all), (5, sh_recv)):
        total(ref, n_tp - 1, send_sem.at[phase]).wait()
    for phase in (2, 4):
        all_sent(send_sem.at[phase]).wait()


def put_out(out_v, st, out, new_state, sem):
    rows = st.shape[0]
    step = rows // 4
    copies = [pltpu.make_async_copy(out_v, out, sem.at[4])]
    for i in range(4):
        some = pl.ds(i * step, step)
        copies.append(pltpu.make_async_copy(st.at[some], new_state.at[some, 0], sem.at[i]))
    for c in copies:
        c.start()
    for c in copies:
        c.wait()


def body(
    tokens, delta_state, mix_gain, w_query, w_key, w_value, w_outgate, w_beta, w_decay, decay_scale, decay_bias,
    head_gain, w_output, ffn_gain, route_ids, route_weights, expert_gate, expert_up, expert_down, shared_gate,
    shared_up, shared_down,
):
    rows, width = tokens.shape
    n_ep, n_tp = lax.axis_size("ep"), lax.axis_size("tp")
    model, dk = w_query.shape
    top = route_ids.shape[1]
    fe = expert_gate.shape[2]
    fs = shared_gate.shape[1]
    slots = 2 * n_ep * n_tp
    block = (n_tp, rows, width)
    spread = (8, 2, rows, width)
    V = pltpu.VMEM
    dma = pltpu.SemaphoreType.DMA
    on_chip = pl.BlockSpec(memory_space=pltpu.VMEM)
    in_hbm = pl.BlockSpec(memory_space=pltpu.HBM)
    out_v, st = pl.pallas_call(
        kernel,
        out_shape=(V(tokens.shape, tokens.dtype), V((rows, dk, dk), F32)),
        in_specs=[in_hbm] * 22,
        out_specs=(on_chip, on_chip),
        scratch_shapes=[
            V(block, BF),
            V((rows, 2 * dk, dk), BF),
            V((model, 4 * dk), BF),
            V((1, model), BF),
            V((1, model), BF),
            pltpu.SMEM((1,), F32),
            pltpu.SMEM((1,), F32),
            V((model,), BF),
            V((dk,), BF),
            V((dk, model), BF),
            V((model,), BF),
            V((8, 2 * width), F32),
            V((top, rows), jnp.int32),
            V((top, rows), F32),
            V((model, fe), BF),
            V((model, fe), BF),
            V((fe, model), BF),
            V((fs, model), BF),
            V((fs, model), BF),
            V((fs, model), BF),
            V(block, BF),
            V((n_tp - 1, rows, width), BF),
            V(spread, BF),
            V(spread, BF),
            V(block, BF),
            V(spread, BF),
            V(spread, BF),
            V(block, BF),
            V((n_tp - 1, rows, width), BF),
            V((slots, rows), BF),
            V((2 * rows, slots), BF),
            V((rows, dk), F32),
            V((rows, dk), F32),
            V((slots, width), BF),
            dma((48,)),
            dma((6,)),
            dma((6,)),
            pltpu.SemaphoreType.REGULAR,
        ],
        compiler_params=pltpu.CompilerParams(
            collective_id=0, has_side_effects=True, vmem_limit_bytes=48 * 1024 * 1024
        ),
        name="layer",
    )(*(v if v.size == 1 else pltpu.with_memory_space_constraint(v, pltpu.HBM) for v in (
        tokens, delta_state, mix_gain, w_query, w_key, w_value, w_outgate, w_beta.T, w_decay.T,
        decay_scale, decay_bias, head_gain, w_output, ffn_gain, route_ids.T,
        route_weights.T, expert_gate, expert_up, expert_down, shared_gate.T, shared_up.T, shared_down,
    )))
    out_v, st = (pltpu.with_memory_space_constraint(v, pltpu.VMEM) for v in (out_v, st))
    return pl.pallas_call(
        put_out,
        out_shape=(
            jax.ShapeDtypeStruct(tokens.shape, tokens.dtype),
            jax.ShapeDtypeStruct(delta_state.shape, delta_state.dtype),
        ),
        in_specs=[on_chip, on_chip],
        out_specs=(in_hbm, in_hbm),
        scratch_shapes=[dma((5,))],
        name="put_out",
    )(out_v, st)


def solution(mesh):
    return jax.shard_map(
        body,
        mesh=mesh,
        in_specs=(
            P("ep", "tp"),
            P("ep", "tp", None, None),
            P(),
            P(None, "tp"),
            P(None, "tp"),
            P(None, "tp"),
            P(None, "tp"),
            P(None, "tp"),
            P(None, "tp"),
            P("tp"),
            P("tp"),
            P(),
            P("tp", None),
            P(),
            P("ep", None),
            P("ep", None),
            P(("ep", "tp"), None, None),
            P(("ep", "tp"), None, None),
            P(("ep", "tp"), None, None),
            P(None, "tp"),
            P(None, "tp"),
            P("tp", None),
        ),
        out_specs=(P("ep", "tp"), P("ep", "tp", None, None)),
        check_vma=False,
    )
```

time: 51.9 us -> 45.3 us (0.87)
  local copies, waits for them, and re-layouts: 4.43 us -> 0 us
  Pallas kernels: 45.3 us -> 43.3 us
    unnamed x2 -> x0, local copies, waits for them, and re-layouts: 4.43 us -> none
    pallas_call x1 -> x2, Pallas kernels: 45.3 us -> 43.3 us  [the longest x1 41.9 us: body(): pl.pallas_call(kernel, out_shape=(V(tokens.shape, tokens.dtype), V((rows,...]
where the time goes in v2:
time: 45.3 us; the launch traced here: 45.2 us
  Pallas kernels  43.3 us (96%)
  between operations  1.94 us (4%)
    pallas_call x1, Pallas kernels, body(): pl.pallas_call(kernel, out_shape=(V(tokens.shape, tokens.dtype), V((rows,...  41.9 us
    pallas_call x1, Pallas kernels, body(): pl.pallas_call(put_out, out_shape=(jax.ShapeDtypeStruct(tokens.shape, tok...  1.36 us

profile of v2, /device:TPU:1, one launch (start us, length us, event | category | flops | bytes accessed | tf_op | source)
XLA Modules:
  0.0 45.2 jit_solution(1073928652253238416)
XLA Ops:
  1.9 41.9 %layer.1 = (bf16[32,128]{1,0:T(8,128)(2,1)S(1)}, f32[32,128,128]{2,1,0:T(8,128)S(1)}) custom-call(bf16[32,128]{1,0:T(8,128)(2,1)} %tokens.1, f32[32,1,128,128]{3,2,1,0:T(8,128)} %state.1, bf16[2048]{0:T(1024)(128)(2,1)} %mix_gain.1, bf16[2048,128]{1,0:T(8,128)(2,1)} %w_query.1, bf16[2048,128]{1,0:T(8,128)(2,1)} %w_key.1, bf16[2048,128]{1,0:T(8,128)(2,1)} %w_value.1, ...), custom_call_target="tpu_custom_call" | custom-call | tf_op jit(solution)/shard_map/layer/pallas_call | solution.py:338
  43.8 1.4 %put_out.1 = (bf16[32,128]{1,0:T(8,128)(2,1)}, f32[32,1,128,128]{3,2,1,0:T(8,128)}) custom-call(bf16[32,128]{1,0:T(8,128)(2,1)S(1)} %get-tuple-element.4.out_v, f32[32,128,128]{2,1,0:T(8,128)S(1)} %get-tuple-element.5.st), custom_call_target="tpu_custom_call" | custom-call | tf_op jit(solution)/shard_map/put_out/pallas_call | solution.py:393

commit v3 on v2

--- a/solution.py
+++ b/solution.py
@@ -58,8 +58,10 @@
     wide2 = 2 * width
 
     barrier = pltpu.get_barrier_semaphore()
-    for d in range(1, n_tp):
+    far_first = [8, 9, 7, 10, 6, 11, 5, 12, 4, 13, 3, 14, 2, 15, 1]
+    for d in far_first:
         pl.semaphore_signal(barrier, inc=1, device_id=(ep, lax.rem(tp + d, n_tp)), device_id_type=MESH)
+    for d in far_first:
         pl.semaphore_signal(barrier, inc=1, device_id=(lax.rem(ep + d, n_ep), tp), device_id_type=MESH)
 
     fetches = []
@@ -69,6 +71,13 @@
         fetches.append(copy)
         copy.start()
         return copy
+
+    def fetch_pieces(pieces, whole):
+        sem = local_sem.at[len(fetches)]
+        for src, dst in pieces:
+            pltpu.make_async_copy(src, dst, sem).start()
+        fetches.append(pltpu.make_async_copy(whole, whole, sem))
+        return fetches[-1]
 
     c_tok = fetch(tokens, tok_all.at[tp])
     c_route = [fetch(ids, idv), fetch(weights, rwv)]
@@ -77,18 +86,20 @@
         fetch(mix_gain, mgain), fetch(w_beta, wb), fetch(w_decay, wd), fetch(decay_scale, dscale),
         fetch(decay_bias, dbias), fetch(head_gain, hgain), fetch(ffn_gain, fgain),
     ]
-    for i, w in enumerate((w_query, w_key, w_value, w_outgate)):
-        c_mix.append(fetch(w, proj_w.at[:, pl.ds(i * dk, dk)]))
+    four = enumerate((w_query, w_key, w_value, w_outgate))
+    c_mix.append(fetch_pieces([(w, proj_w.at[:, pl.ds(i * dk, dk)]) for i, w in four], proj_w))
     c_mix.append(fetch(w_output, wo))
     c_sh = [fetch(s_gate, sg), fetch(s_up, su), fetch(s_down, sd)]
-    c_ex = []
     z_from = [lax.rem(z + 8 - ZO[a], 8) for a in range(8)]
     z_to = [lax.rem(z + ZO[a], 8) for a in range(8)]
-    for a in range(8):
-        here, there = pl.ds(a * wide2, wide2), pl.ds(pl.multiple_of(z_from[a] * wide2, wide2), wide2)
-        c_ex += [fetch(e_gate.at[0, there], eg.at[here]), fetch(e_up.at[0, there], eu.at[here])]
-        there = pl.ds(pl.multiple_of(z_to[a] * wide2, wide2), wide2)
-        c_ex.append(fetch(e_down.at[0, :, there], ed.at[:, here]))
+    here = [pl.ds(a * wide2, wide2) for a in range(8)]
+    from_z = [pl.ds(pl.multiple_of(v * wide2, wide2), wide2) for v in z_from]
+    to_z = [pl.ds(pl.multiple_of(v * wide2, wide2), wide2) for v in z_to]
+    c_ex = [
+        fetch_pieces([(e_gate.at[0, from_z[a]], eg.at[here[a]]) for a in range(8)], eg),
+        fetch_pieces([(e_up.at[0, from_z[a]], eu.at[here[a]]) for a in range(8)], eu),
+        fetch_pieces([(e_down.at[0, :, to_z[a]], ed.at[:, here[a]]) for a in range(8)], ed),
+    ]
 
     def total(ref, count, sem):
         return pltpu.make_async_copy(ref.at[pl.ds(0, count)], ref.at[pl.ds(0, count)], sem)
@@ -98,8 +109,6 @@
             src, dst, send_sem.at[phase], recv_sem.at[phase],
             device_id=(ep, lax.rem(tp + d, n_tp)), device_id_type=MESH,
         ).start()
-
-    far_first = [8, 9, 7, 10, 6, 11, 5, 12, 4, 13, 3, 14, 2, 15, 1]
 
     c_tok.wait()
     pl.semaphore_wait(barrier, n_ep + n_tp - 2)
@@ -161,13 +170,13 @@
         fgain8[i : i + 1, :] = fgain_row[:, i * wide2 : (i + 1) * wide2]
     total(tok_all, n_tp - 1, recv_sem.at[0]).wait()
 
-    def normed_rows(blocks, gain_row):
+    def gained(blocks, gain_row):
         values = jnp.concatenate(blocks, axis=1).astype(F32)
         squares = jnp.mean(values * values, axis=1, keepdims=True)
-        return (values * lax.rsqrt(squares + EPS) * gain_row).astype(BF)
-
-    normed = normed_rows([tok_all[t] for t in range(n_tp)], row(mgain))
-    projected = dot(normed, proj_w[...]).astype(BF).astype(F32)
+        return (values * gain_row).astype(BF), lax.rsqrt(squares + EPS)
+
+    rows_in, scale = gained([tok_all[t] for t in range(n_tp)], row(mgain))
+    projected = (dot(rows_in, proj_w[...]) * scale).astype(BF).astype(F32)
     query, key, value, gate = (projected[:, i * dk : (i + 1) * dk] for i in range(4))
 
     def unit(v):
@@ -191,9 +200,9 @@
             both = dot(left, st_split[s])
             k_read[s : s + 1, :] = both[i : i + 1] + both[16 + i : 17 + i]
             q_read[s : s + 1, :] = both[8 + i : 9 + i] + both[24 + i : 25 + i]
-    wide = normed.astype(F32)
-    beta = jax.nn.sigmoid(jnp.sum(wide * wb[...].astype(F32), axis=1, keepdims=True))
-    decay_in = jnp.sum(wide * wd[...].astype(F32), axis=1, keepdims=True) + dbias[0]
+    wide = rows_in.astype(F32)
+    beta = jax.nn.sigmoid(jnp.sum(wide * wb[...].astype(F32), axis=1, keepdims=True) * scale)
+    decay_in = jnp.sum(wide * wd[...].astype(F32), axis=1, keepdims=True) * scale + dbias[0]
     softplus = jnp.maximum(decay_in, 0.0) + jnp.log(1.0 + jnp.exp(-jnp.abs(decay_in)))
     decay = jnp.exp(-dscale[0] * softplus)
     written = beta * (value - decay * k_read[...])
@@ -265,8 +274,8 @@
     for c in range(2):
         blocks[14 + c] = jnp.where(own_block & (core == c), own_disp, blocks[14 + c])
     gain_from = jnp.concatenate([fgain8[pl.ds(z_from[a], 1), :] for a in range(8)], axis=1)
-    routed_rows = normed_rows(blocks, gain_from)
-    hidden = (silu(dot(routed_rows, eg[...])) * dot(routed_rows, eu[...])).astype(BF)
+    rows_in, scale = gained(blocks, gain_from)
+    hidden = (silu(dot(rows_in, eg[...]) * scale) * (dot(rows_in, eu[...]) * scale)).astype(BF)
     results = dot(hidden, ed[...])
     for a in range(8):
         for c in range(2):
@@ -277,8 +286,8 @@
     for c in c_sh:
         c.wait()
     total(res_all, n_tp - 1, recv_sem.at[3]).wait()
-    normed_ffn = normed_rows([res_all[t] for t in range(n_tp)], fgain_row)
-    hidden_shared = (silu(dot_nt(normed_ffn, sg[...])) * dot_nt(normed_ffn, su[...])).astype(BF)
+    rows_in, scale = gained([res_all[t] for t in range(n_tp)], fgain_row)
+    hidden_shared = (silu(dot_nt(rows_in, sg[...]) * scale) * (dot_nt(rows_in, su[...]) * scale)).astype(BF)
     shared = dot(hidden_shared, sd[...])
     own_shared = jnp.zeros((rows, width), F32)
     for t in range(n_tp):
@@ -307,14 +316,13 @@
 def put_out(out_v, st, out, new_state, sem):
     rows = st.shape[0]
     step = rows // 4
-    copies = [pltpu.make_async_copy(out_v, out, sem.at[4])]
+    c_out = pltpu.make_async_copy(out_v, out, sem.at[1])
     for i in range(4):
         some = pl.ds(i * step, step)
-        copies.append(pltpu.make_async_copy(st.at[some], new_state.at[some, 0], sem.at[i]))
-    for c in copies:
-        c.start()
-    for c in copies:
-        c.wait()
+        pltpu.make_async_copy(st.at[some], new_state.at[some, 0], sem.at[0]).start()
+    c_out.start()
+    pltpu.make_async_copy(st, new_state.at[:, 0], sem.at[0]).wait()
+    c_out.wait()
 
 
 def body(
@@ -375,7 +383,7 @@
             V((rows, dk), F32),
             V((rows, dk), F32),
             V((slots, width), BF),
-            dma((48,)),
+            dma((19,)),
             dma((6,)),
             dma((6,)),
             pltpu.SemaphoreType.REGULAR,
@@ -398,7 +406,7 @@
         ),
         in_specs=[on_chip, on_chip],
         out_specs=(in_hbm, in_hbm),
-        scratch_shapes=[dma((5,))],
+        scratch_shapes=[dma((2,))],
         name="put_out",
     )(out_v, st)
 

time: 45.3 us -> 44.7 us (0.987)
  Pallas kernels: 43.3 us -> 42.6 us
    pallas_call x1, Pallas kernels: 41.9 us -> 41.3 us  [body(): pl.pallas_call(kernel, out_shape=(V(tokens.shape, tokens.dtype), V((rows,...]
where the time goes in v3:
time: 44.7 us; the launch traced here: 44.6 us
  Pallas kernels  42.6 us (95%)
  between operations  1.94 us (4%)
    pallas_call x1, Pallas kernels, body(): pl.pallas_call(kernel, out_shape=(V(tokens.shape, tokens.dtype), V((rows,...  41.3 us
    pallas_call x1, Pallas kernels, body(): pl.pallas_call(put_out, out_shape=(jax.ShapeDtypeStruct(tokens.shape, tok...  1.33 us

profile of v3, /device:TPU:1, one launch (start us, length us, event | category | flops | bytes accessed | tf_op | source)
XLA Modules:
  0.0 44.6 jit_solution(17405471823745899814)
XLA Ops:
  1.9 41.3 %layer.1 = (bf16[32,128]{1,0:T(8,128)(2,1)S(1)}, f32[32,128,128]{2,1,0:T(8,128)S(1)}) custom-call(bf16[32,128]{1,0:T(8,128)(2,1)} %tokens.1, f32[32,1,128,128]{3,2,1,0:T(8,128)} %state.1, bf16[2048]{0:T(1024)(128)(2,1)} %mix_gain.1, bf16[2048,128]{1,0:T(8,128)(2,1)} %w_query.1, bf16[2048,128]{1,0:T(8,128)(2,1)} %w_key.1, bf16[2048,128]{1,0:T(8,128)(2,1)} %w_value.1, ...), custom_call_target="tpu_custom_call" | custom-call | tf_op jit(solution)/shard_map/layer/pallas_call | solution.py:346
  43.3 1.3 %put_out.1 = (bf16[32,128]{1,0:T(8,128)(2,1)}, f32[32,1,128,128]{3,2,1,0:T(8,128)}) custom-call(bf16[32,128]{1,0:T(8,128)(2,1)S(1)} %get-tuple-element.4.out_v, f32[32,128,128]{2,1,0:T(8,128)S(1)} %get-tuple-element.5.st), custom_call_target="tpu_custom_call" | custom-call | tf_op jit(solution)/shard_map/put_out/pallas_call | solution.py:401

commit v4 on v3

--- a/solution.py
+++ b/solution.py
@@ -30,6 +30,14 @@
 
 ZO = (4, 3, 5, 2, 6, 1, 7, 0)
 RO = (2, 1, 3, 0)
+
+
+def hops(place):
+    a, i = place
+    return min(ZO[a], 8 - ZO[a]) + sum(min(RO[k], 4 - RO[k]) for k in (i // 4, i % 4))
+
+
+BY_HOPS = sorted(((a, i) for i in range(16) for a in range(8)), key=lambda place: -hops(place))[:-1]
 
 
 def ring(i, n):
@@ -244,16 +252,9 @@
                 device_id=(to_ep[i], dev_tp), device_id_type=MESH,
             ).start()
 
-        @pl.loop(0, 7)
-        def _(a):
-            dev_tp = lax.rem(z + ring(a, 8), 8) * 2
-            for i in range(16):
-                for c in range(2):
-                    send(a, c, i, dev_tp + c)
-
-        for i in range(15):
+        for a, i in BY_HOPS:
             for c in range(2):
-                send(7, c, i, 2 * z + c)
+                send(a, c, i, 2 * z_to[a] + c)
         send(7, 1 - core, 15, 2 * z + 1 - core)
 
     def all_sent(sem):

time: 44.7 us -> 44.4 us (level)
  no operation moved by 1% of the time
where the time goes in v4:
time: 44.4 us; the launch traced here: 44.3 us
  Pallas kernels  42.3 us (95%)
  between operations  1.94 us (4%)
    pallas_call x1, Pallas kernels, body(): pl.pallas_call(kernel, out_shape=(V(tokens.shape, tokens.dtype), V((rows,...  41 us
    pallas_call x1, Pallas kernels, body(): pl.pallas_call(put_out, out_shape=(jax.ShapeDtypeStruct(tokens.shape, tok...  1.33 us

profile of v4, /device:TPU:1, one launch (start us, length us, event | category | flops | bytes accessed | tf_op | source)
XLA Modules:
  0.0 44.3 jit_solution(9946540249769863119)
XLA Ops:
  1.9 41.0 %layer.1 = (bf16[32,128]{1,0:T(8,128)(2,1)S(1)}, f32[32,128,128]{2,1,0:T(8,128)S(1)}) custom-call(bf16[32,128]{1,0:T(8,128)(2,1)} %tokens.1, f32[32,1,128,128]{3,2,1,0:T(8,128)} %state.1, bf16[2048]{0:T(1024)(128)(2,1)} %mix_gain.1, bf16[2048,128]{1,0:T(8,128)(2,1)} %w_query.1, bf16[2048,128]{1,0:T(8,128)(2,1)} %w_key.1, bf16[2048,128]{1,0:T(8,128)(2,1)} %w_value.1, ...), custom_call_target="tpu_custom_call" | custom-call | tf_op jit(solution)/shard_map/layer/pallas_call | solution.py:347
  43.0 1.3 %put_out.1 = (bf16[32,128]{1,0:T(8,128)(2,1)}, f32[32,1,128,128]{3,2,1,0:T(8,128)}) custom-call(bf16[32,128]{1,0:T(8,128)(2,1)S(1)} %get-tuple-element.4.out_v, f32[32,128,128]{2,1,0:T(8,128)S(1)} %get-tuple-element.5.st), custom_call_target="tpu_custom_call" | custom-call | tf_op jit(solution)/shard_map/put_out/pallas_call | solution.py:402
